TPU v7x, 256 devices: a 4x2x16 block of a 4x16x16 slice. The times are simulated.
256 devices in a mesh: grp: 2 (over y), sp: 16 (over z), tp: 8 (over x, core).
Axes of the slice: x: 4, y: 2, z: 16, core: 2. Of those that a mesh axis runs over, the one named last changes fastest.
The devices are a block of a 4x16x16 slice.
Arguments:
- tokens: bfloat16 [16384, 4096], P(('grp', 'sp', 'tp')), parts along dimension 0, may hold values from -6 to 6
- norm_gain: float32 [4096], replicated, may hold values from 0.1 to 1.9
- query_diff: bfloat16 [4096, 2048], P('sp', 'tp'), may hold values from -1.25 to 1.25
- key_diff: bfloat16 [4096, 2048], P('sp', 'tp'), may hold values from -1.25 to 1.25
- value_diff: bfloat16 [4096, 2048], P('sp', 'tp'), may hold values from -0.09375 to 0.09375
- lam: float32 [8], P('tp'), may hold values from 0.3 to 0.8
- output_norm_gain: float32 [256], replicated, may hold values from 0.1 to 1.9
- query_win: bfloat16 [4096, 2048], P('sp', 'tp'), may hold values from -1.25 to 1.25
- keyval_win: bfloat16 [4, 4096, 256], P(None, 'sp'), may hold values from -1.25 to 1.25
- sink: float32 [16], P('tp'), may hold values from 4 to 7
- proj_diff: bfloat16 [2048, 4096], P('tp'), may hold values from -0.125 to 0.125
- proj_win: bfloat16 [2048, 4096], P('tp'), may hold values from -0.79296875 to 0.79296875
Outputs:
- mixed: bfloat16 [16384, 4096], P(('grp', 'sp', 'tp')), parts along dimension 0
There are 2 independent parts, one for each index of `grp`. A program takes and returns all parts, laid end to end along the dimension named above; an argument that names none is the same for every part. Nothing has to cross between parts.
All inputs are finite; a program needn't handle non-finite values.
Results may differ from a plain program's by a relative error of at most 0.015.
Values may be sent and summed in bfloat16 or wider, within the bound.
A program may use at most 128 MiB of HBM per device.

v0:
```python
import math
import jax
import jax.numpy as jnp
from jax import lax
from jax.sharding import Mesh
from jax.sharding import PartitionSpec as P

HEAD = 128
WIN_HEADS = 16
KV_HEADS = 4
WINDOW = 128
VDIM = 256
TP = ("tp_0", "tp_1")
GRP_SP_TP = ("grp", "sp", "tp_0", "tp_1")
EPS = 1e-06


def in_order(parts, dim):
    shape = list(parts.shape[1:])
    shape[dim] *= parts.shape[0]
    return jnp.moveaxis(parts, 0, dim).reshape(shape)


def stacked_from(x, axes, order):
    parts = x[None]
    for k in order:
        parts = lax.all_gather(parts, axes[k], axis=0, tiled=True)
    block = [lax.axis_size(axes[k]) for k in reversed(order)]
    parts = parts.reshape(*block, *x.shape)
    turned = sorted(range(len(order)), key=lambda place: order[len(order) - 1 - place])
    return parts.transpose(*turned, *range(len(order), parts.ndim)).reshape(-1, *x.shape)


def gathered_by_axis(x, axes, order, dim):
    return in_order(stacked_from(x, axes, order), dim)


def side_by_side(arrays, axis, dim, along):
    both = jnp.concatenate(arrays, axis=along)
    out, at, done = (lax.all_gather(both, axis, axis=dim, tiled=True), 0, [])
    for a in arrays:
        done.append(lax.slice_in_dim(out, at, at + a.shape[along], axis=along))
        at += a.shape[along]
    return tuple(done)


def padded_2(x, sides, width):
    for axis, dim in sides:
        devices, length = (lax.axis_size(axis), x.shape[dim])
        up = [(i, (i + 1) % devices) for i in range(devices - 1)]
        down = [(j, i) for i, j in up]
        last = lax.slice_in_dim(x, length - width, length, axis=dim)
        first = lax.slice_in_dim(x, 0, width, axis=dim)
        before = lax.ppermute(last, axis, up)
        after = lax.ppermute(first, axis, down)
        x = jnp.concatenate([before, x, after], axis=dim)
    return x


def root_mean_square_rows(values, gain):
    return values * lax.rsqrt(jnp.mean(values * values, axis=-1, keepdims=True) + EPS) * gain


def body(
    tokens,
    norm_gain,
    query_diff,
    key_diff,
    value_diff,
    lam,
    output_norm_gain,
    query_win,
    keyval_win,
    sink,
    proj_diff,
    proj_win,
):
    normed = root_mean_square_rows(tokens.astype(jnp.float32), norm_gain).astype(jnp.bfloat16)
    heads_diff = lam.shape[0]
    heads_win = sink.shape[0]
    group = WIN_HEADS // KV_HEADS
    kv_index = lax.axis_index(TP) * heads_win // group
    kv_local = lax.dynamic_index_in_dim(keyval_win, kv_index, 0, keepdims=False)
    pieces = [query_diff, key_diff, value_diff, query_win, kv_local]
    stacked = jnp.concatenate(pieces, axis=1)
    rows_all = gathered_by_axis(normed, TP, (0, 1), 0)
    projected = jnp.dot(
        rows_all,
        lax.all_gather(stacked, "sp", axis=0, tiled=True),
        preferred_element_type=jnp.float32,
    )
    projected = projected.astype(jnp.bfloat16)
    output_list = []
    offset = 0
    for piece in pieces:
        output_list.append(projected[:, offset : offset + piece.shape[1]])
        offset = offset + piece.shape[1]
    q_diff, k_diff, v_diff, q_win, kv_win = output_list
    tok = projected.shape[0]
    scale = HEAD ** (-0.5)
    q_four = q_diff.reshape(tok, heads_diff, 2, HEAD)
    start_state = (
        jnp.full((heads_diff, 2, tok), -jnp.inf, jnp.float32),
        jnp.zeros((heads_diff, 2, tok), jnp.float32),
        jnp.zeros((heads_diff, 2, tok, VDIM), jnp.float32),
    )
    carry = start_state
    keys, values = side_by_side((k_diff, v_diff), "sp", 0, 1)
    rows = keys.shape[0]
    step = math.gcd(rows, 1024)
    key_blocks = keys.reshape(rows // step, step, heads_diff, 2, HEAD)
    value_blocks = values.reshape(rows // step, step, heads_diff, VDIM)

    def one(state, block):
        top, total, acc = state
        key_part, value_part = block
        scores = (
            jnp.einsum("qhmd,khmd->hmqk", q_four, key_part, preferred_element_type=jnp.float32)
            * scale
        )
        new_top = jnp.maximum(top, jnp.max(scores, axis=-1))
        expo = jnp.exp(scores - new_top[..., None])
        fade = jnp.exp(top - new_top)
        total = total * fade + jnp.sum(expo, axis=-1)
        acc = acc * fade[..., None] + jnp.einsum(
            "hmqk,khe->hmqe",
            expo.astype(jnp.bfloat16),
            value_part,
            preferred_element_type=jnp.float32,
        )
        return ((new_top, total, acc), None)

    carry, unused = lax.scan(one, carry, (key_blocks, value_blocks))
    top, total, acc = carry
    attention_maps = acc / total[..., None]
    difference_output = attention_maps[:, 0] - lam[:, None, None] * attention_maps[:, 1]
    differential_output = root_mean_square_rows(difference_output, output_norm_gain).astype(
        jnp.bfloat16
    )
    differential_output = jnp.transpose(differential_output, (1, 0, 2)).reshape(
        tok, heads_diff * VDIM
    )
    padded = padded_2(kv_win, (("sp", 0),), WINDOW)
    nblocks = tok // WINDOW
    blocks = padded.reshape(nblocks + 2, WINDOW, 2 * HEAD)
    band = jnp.concatenate([blocks[:-2], blocks[1:-1], blocks[2:]], axis=1)
    q_blocks = q_win.reshape(nblocks, WINDOW, heads_win, HEAD)
    scores = (
        jnp.einsum("nqhd,nkd->nhqk", q_blocks, band[..., :HEAD], preferred_element_type=jnp.float32)
        * scale
    )
    q_index = jnp.arange(WINDOW)
    k_index = jnp.arange(3 * WINDOW)
    relative = k_index[None, :] - WINDOW - q_index[:, None]
    first_key = lax.axis_index("sp") * tok - WINDOW
    key_pos = first_key + jnp.arange(nblocks)[:, None] * WINDOW + k_index[None, :]
    inside = (key_pos >= 0) & (key_pos < tok * lax.axis_size("sp"))
    valid = (jnp.abs(relative) <= WINDOW)[None] & inside[:, None, :]
    scores = jnp.where(valid[:, None], scores, -jnp.inf)
    sink_logit = sink[None, :, None, None]
    top_win = jnp.maximum(jnp.max(scores, axis=-1, keepdims=True), sink_logit)
    expo = jnp.exp(scores - top_win)
    weights = expo / (jnp.sum(expo, axis=-1, keepdims=True) + jnp.exp(sink_logit - top_win))
    y_win = jnp.einsum(
        "nhqk,nkd->nqhd",
        weights.astype(jnp.bfloat16),
        band[..., HEAD:],
        preferred_element_type=jnp.float32,
    ).astype(jnp.bfloat16)
    y_win = y_win.reshape(tok, heads_win * HEAD)
    summed = jnp.dot(differential_output, proj_diff, preferred_element_type=jnp.float32)
    return lax.psum_scatter(
        (summed + jnp.dot(y_win, proj_win, preferred_element_type=jnp.float32)).astype(
            jnp.bfloat16
        ),
        TP,
        scatter_dimension=0,
        tiled=True,
    )


def solution(mesh):
    torus = Mesh(
        mesh.devices.reshape(mesh.shape["grp"], mesh.shape["sp"], 4, 2),
        ("grp", "sp", "tp_0", "tp_1"),
    )
    return jax.shard_map(
        body,
        mesh=torus,
        in_specs=(
            P(GRP_SP_TP, None),
            P(),
            P("sp", TP),
            P("sp", TP),
            P("sp", TP),
            P(TP),
            P(),
            P("sp", TP),
            P(None, "sp", None),
            P(TP),
            P(TP, None),
            P(TP, None),
        ),
        out_specs=P(GRP_SP_TP, None),
        check_vma=False,
    )
```

profile of v0, /device:TPU:40, one launch (start us, length us, event | category | flops | bytes accessed | tf_op | source)
XLA Modules:
  0.0 442.2 jit_solution(13832787000681153917)
XLA Ops:
  8.0 2.0 fusion.24
  10.2 50.1 %all-gather.12.cloned.1.call-done = bf16[256,4096]{1,0:T(8,128)(2,1)} async-done(((bf16[64,4096]{1,0:T(8,128)(2,1)}), bf16[256,4096]{1,0:T(8,128)(2,1)}) %all-gather.12.cloned.1.call-update) | async-done | bytes 2097168 | tf_op jit(solution)/shard_map/all_gather | solution.py:27
  62.5 22.3 %all-gather.6.cloned.1.call-done = bf16[8,64,4096]{2,1,0:T(8,128)(2,1)} async-done(((bf16[4,64,4096]{2,1,0:T(8,128)(2,1)}), bf16[8,64,4096]{2,1,0:T(8,128)(2,1)}) %all-gather.6.cloned.1.call-update) | async-done | bytes 4194320 | tf_op jit(solution)/shard_map/all_gather | solution.py:27
  84.8 4.7 %copy.38 = bf16[4,2,64,4096]{3,2,1,0:T(8,128)(2,1)} copy(bf16[4,2,64,4096]{3,2,0,1:T(8,128)(2,1)} %bitcast.110) | data formatting | bytes 8388608 | tf_op jit(solution)/shard_map/transpose | solution.py:31
  89.5 123.6 %all-gather.8.cloned.1.call-done = bf16[4096,1280]{1,0:T(8,128)(2,1)} async-done(((bf16[256,1280]{1,0:T(8,128)(2,1)}), bf16[4096,1280]{1,0:T(8,128)(2,1)}) %all-gather.8.cloned.1.call-update) | async-done | bytes 10485776 | tf_op jit(solution)/shard_map/all_gather | solution.py:89
  213.0 10.4 %convolution_convert_fusion = bf16[512,1280]{1,0:T(8,128)(2,1)S(1)} fusion(bf16[512,4096]{1,0:T(8,128)(2,1)} %bitcast.111, bf16[4096,1280]{1,0:T(8,128)(2,1)} %all-gather.8.cloned.1.call-done), kind=kOutput, calls=%fused_computation.26 | convolution fusion | flops 5369364480 | bytes 15990784 | tf_op jit(solution)/shard_map/dot_general | solution.py:87
  227.0 1.4 collective-permute-start
  228.4 1.5 collective-permute-start.1
  231.3 3.5 collective-permute-done.1
  236.4 90.3 %all-gather.10.cloned.1.call-done = bf16[8192,512]{1,0:T(8,128)(2,1)} async-done(((bf16[512,512]{1,0:T(8,128)(2,1)}), bf16[8192,512]{1,0:T(8,128)(2,1)}) %all-gather.10.cloned.1.call-update) | async-done | bytes 8388624 | tf_op jit(solution)/shard_map/all_gather | solution.py:40
  326.7 5.7 %fusion.39 = (bf16[8192,256]{1,0:T(8,128)(2,1)}, bf16[8192,256]{1,0:T(8,128)(2,1)}) fusion(bf16[8192,512]{1,0:T(8,128)(2,1)} %all-gather.10.cloned.1.call-done), kind=kLoop, calls=%fused_computation.73 | loop fusion | bytes 16777216 | tf_op jit(solution)/shard_map/slice | solution.py:42
  332.4 6.9 %reshape.210 = bf16[8,1024,1,2,128]{4,3,1,0,2:T(2,128)(2,1)} reshape(bf16[8192,256]{1,0:T(8,128)(2,1)} %get-tuple-element.116) | data formatting | bytes 8388608 | tf_op jit(solution)/shard_map/reshape | solution.py:111
  339.3 47.5 %while.15 = (s32[]{:T(128)}, f32[1,2,512]{2,1,0:T(2,128)S(1)}, f32[1,2,512]{2,1,0:T(2,128)S(1)}, f32[1,2,512,256]{3,2,1,0:T(8,128)}, bf16[8,1024,1,2,128]{4,3,1,...) while((s32[]{:T(128)}, f32[1,2,512]{2,1,0:T(2,128)S(1)}, ...), condition=%wide.region_4.5_spmd.clone, body=%wide.region_1.4_spmd.clone.sunk | while | flops 814487552 | bytes 25493680 | solution.py:133
  342.2 2.1 fusion.56
  348.1 2.1 fusion.56
  354.1 2.1 fusion.56
  360.0 2.1 fusion.56
  365.9 2.1 fusion.56
  371.9 2.1 fusion.56
  377.8 2.1 fusion.56
  383.8 2.1 fusion.56
  386.8 1.4 broadcast_divide_fusion
  390.0 3.3 add_convert_fusion
  393.4 42.3 %reduce-scatter.2.cloned.1.call-done = bf16[64,4096]{1,0:T(8,128)(2,1)} async-done(((bf16[512,4096]{1,0:T(8,128)(2,1)}), bf16[64,4096]{1,0:T(8,128)(2,1)}) %reduce-scatter.2.cloned.1.call-update) | async-done | bytes 524304 | tf_op jit(solution)/shard_map/reduce_scatter | solution.py:172
  (145 shorter events, 41.7 us)
Async XLA Ops:
  6.5 381.9 %copy-start = (bf16[256,4096]{1,0:T(8,128)(2,1)S(1)}, bf16[256,4096]{1,0:T(8,128)(2,1)}, u32[]{:S(2)}) copy-start(bf16[256,4096]{1,0:T(8,128)(2,1)} %param.24) | copy-start | bytes 6291460
  6.6 54.0 %copy-start.7 = (bf16[256,256]{1,0:T(8,128)(2,1)S(1)}, bf16[256,256]{1,0:T(8,128)(2,1)}, u32[]{:S(2)}) copy-start(bf16[256,256]{1,0:T(8,128)(2,1)} %param.16) | copy-start | bytes 393220
  6.6 54.0 %copy-start.8 = (bf16[256,256]{1,0:T(8,128)(2,1)S(1)}, bf16[256,256]{1,0:T(8,128)(2,1)}, u32[]{:S(2)}) copy-start(bf16[256,256]{1,0:T(8,128)(2,1)} %param.17) | copy-start | bytes 393220
  6.6 54.0 %copy-start.9 = (bf16[256,256]{1,0:T(8,128)(2,1)S(1)}, bf16[256,256]{1,0:T(8,128)(2,1)}, u32[]{:S(2)}) copy-start(bf16[256,256]{1,0:T(8,128)(2,1)} %param.18) | copy-start | bytes 393220
  6.6 54.0 %copy-start.10 = (bf16[256,256]{1,0:T(8,128)(2,1)S(1)}, bf16[256,256]{1,0:T(8,128)(2,1)}, u32[]{:S(2)}) copy-start(bf16[256,256]{1,0:T(8,128)(2,1)} %param.21) | copy-start | bytes 393220
  6.6 53.8 %all-gather.12.cloned.1.call-start = ((), (), s32[]{:S(2)}) async-start(), calls=%async_computation.5 | async-start | bytes 2621440 | tf_op jit(solution)/shard_map/all_gather | solution.py:27
  10.1 74.7 %all-gather.6.cloned.1.call-start = ((), (), s32[]{:S(2)}) async-start(), calls=%async_computation.1 | async-start | bytes 6291456 | tf_op jit(solution)/shard_map/all_gather | solution.py:27
  60.4 152.6 %all-gather.8.cloned.1.call-start = ((), (), s32[]{:S(2)}) async-start(), calls=%async_computation.2 | async-start | bytes 11141120 | tf_op jit(solution)/shard_map/all_gather | solution.py:89
  62.4 264.2 %all-gather.10.cloned.1.call-start = ((), (), s32[]{:S(2)}) async-start(), calls=%async_computation.3 | async-start | bytes 8912896 | tf_op jit(solution)/shard_map/all_gather | solution.py:40
  223.4 5.0 %copy-start.2 = (bf16[512,1280]{1,0:T(8,128)(2,1)}, bf16[512,1280]{1,0:T(8,128)(2,1)S(1)}, u32[]{:S(2)}) copy-start(bf16[512,1280]{1,0:T(8,128)(2,1)S(1)} %convolution_convert_fusion) | copy-start | bytes 3932164
  224.4 211.3 %reduce-scatter.2.cloned.1.call-start = ((), (), s32[]{:S(2)}) async-start(), calls=%async_computation.4 | async-start | bytes 4718592 | tf_op jit(solution)/shard_map/reduce_scatter | solution.py:172
  227.0 8.3 %copy-start.12 = (f32[2]{0:T(128)S(1)}, f32[2]{0:T(128)}, u32[]{:S(2)}) copy-start(f32[2]{0:T(128)} %param.23) | copy-start | bytes 28
  227.0 4.4 collective-permute-start
  228.4 6.4 %collective-permute-start.1 = (bf16[128,256]{1,0:T(8,128)(2,1)}, bf16[128,256]{1,0:T(8,128)(2,1)S(1)}, u32[]{:S(2)}, u32[]{:S(2)}) collective-permute-start(bf16[128,256]{1,0:T(8,128)(2,1)} %get-tuple-element.121), channel_id=1, source_target_pairs={{8,0},{16,8},{24,16},{32,24},{40,32},{48,40},{56,48},{64,56},{72,6... | collective-permute-start | bytes 196616 | tf_op jit(solution)/shard_map/ppermute | solution.py:55
  229.9 5.0 %copy-start.6 = (pred[4,128,384]{1,2,0:T(8,128)(4,1)S(1)}, pred[4,128,384]{1,2,0:T(8,128)(4,1)}, u32[]{:S(2)}) copy-start(pred[4,128,384]{1,2,0:T(8,128)(4,1)} %broadcast_and_fusion) | copy-start | bytes 589828
  339.3 49.1 %copy-start.11 = (f32[256]{0:T(256)S(1)}, f32[256]{0:T(256)}, u32[]{:S(2)}) copy-start(f32[256]{0:T(256)} %param.20) | copy-start | bytes 3076
  346.7 1.5 copy-start.3
  352.6 1.5 copy-start.3
  358.5 1.5 copy-start.3
  364.5 1.5 copy-start.3
  370.4 1.5 copy-start.3
  376.4 1.5 copy-start.3
  382.3 1.5 copy-start.3
  388.4 1.6 copy-start.1
  (10 other events, 10.2 us)
Sparse Core Ops, SparseCore 0:
  10.3 50.0 all-gather.11
  62.2 22.5 all-gather.5
  86.6 126.3 all-gather.7
  224.5 102.1 all-gather.9
  393.5 42.0 reduce-scatter.1
where the time goes:
time: 443 us; the launch traced here: 442 us
  waiting for transfers between devices  332 us (75%)
  local copies, waits for them, and re-layouts  41.4 us (9%)
  matrix products  38.1 us (9%)
  between operations  14.2 us (3%)
  other arithmetic  12.5 us (3%)
    all_gather x1, waiting for transfers between devices, body(): lax.all_gather(stacked, 'sp', axis=0, tiled=True)  124 us
    all_gather x1, waiting for transfers between devices, side_by_side(): out, at, done = (lax.all_gather(both, axis, axis=dim, tiled=True), 0, [])  90.3 us
    all_gather x2, waiting for transfers between devices, stacked_from(): parts = lax.all_gather(parts, axes[k], axis=0, tiled=True)  72.4 us
    reduce_scatter x1, waiting for transfers between devices, body(): lax.psum_scatter((summed + jnp.dot(y_win, proj_win, preferred_element_typ...  42.3 us
    dot_general x8, matrix products, one(): jnp.einsum('hmqk,khe->hmqe', expo.astype(jnp.bfloat16), value_part, prefe...  16.5 us
    dynamic_slice x8, local copies, waits for them, and re-layouts, body(): carry, unused = lax.scan(one, carry, (key_blocks, value_blocks))  11.2 us
    dot_general x1, matrix products, body(): jnp.dot(rows_all, lax.all_gather(stacked, 'sp', axis=0, tiled=True), pref...  10.4 us
  transfers between devices with their start and end apart: 7, of which 6 were waited for; matrix products, arithmetic and copies ran while one was open for 2% of the time, Pallas kernels for 0%

commit v1 on v0

--- a/solution.py
+++ b/solution.py
@@ -13,6 +13,25 @@
 TP = ("tp_0", "tp_1")
 GRP_SP_TP = ("grp", "sp", "tp_0", "tp_1")
 EPS = 1e-06
+
+
+def collect(value, axis, dim):
+    size, place, rows = (lax.axis_size(axis), lax.axis_index(axis), value.shape[dim])
+    right = [(i, (i + 1) % size) for i in range(size)]
+    backward = [(i, (i - 1) % size) for i in range(size)]
+    out = jnp.zeros((*value.shape[:dim], size * rows, *value.shape[dim + 1 :]), value.dtype)
+    out = lax.dynamic_update_slice_in_dim(out, value, place * rows, axis=dim)
+    from_left = from_right = value
+    half = size // 2
+    for hop in range(1, half + 1):
+        from_left = lax.ppermute(from_left, axis, right)
+        out = lax.dynamic_update_slice_in_dim(out, from_left, (place - hop) % size * rows, axis=dim)
+        if hop < size - half:
+            from_right = lax.ppermute(from_right, axis, backward)
+            out = lax.dynamic_update_slice_in_dim(
+                out, from_right, (place + hop) % size * rows, axis=dim
+            )
+    return out
 
 
 def in_order(parts, dim):
@@ -84,11 +103,7 @@
     pieces = [query_diff, key_diff, value_diff, query_win, kv_local]
     stacked = jnp.concatenate(pieces, axis=1)
     rows_all = gathered_by_axis(normed, TP, (0, 1), 0)
-    projected = jnp.dot(
-        rows_all,
-        lax.all_gather(stacked, "sp", axis=0, tiled=True),
-        preferred_element_type=jnp.float32,
-    )
+    projected = jnp.dot(rows_all, collect(stacked, "sp", 0), preferred_element_type=jnp.float32)
     projected = projected.astype(jnp.bfloat16)
     output_list = []
     offset = 0

time: 443 us -> 412 us (0.930)
  waiting for transfers between devices: 332 us -> 207 us
  starting transfers between devices: 3.23 us -> 46.6 us
  matrix products: 38.1 us -> 72.7 us
  local copies, waits for them, and re-layouts: 41.4 us -> 57.8 us
    all_gather x1 -> x0, waiting for transfers between devices: 124 us -> none  [body(): lax.all_gather(stacked, 'sp', axis=0, tiled=True)]
    ppermute x0 -> x15, waiting for transfers between devices: none -> 77.6 us  [the longest x8 66.2 us: collect(): from_left = lax.ppermute(from_left, axis, right)]
    all_gather x2, waiting for transfers between devices: 72.4 us -> 0.01 us  [stacked_from(): parts = lax.all_gather(parts, axes[k], axis=0, tiled=True)]
    ppermute x0 -> x15, starting transfers between devices: none -> 43.4 us  [the longest x7 40.5 us: collect(): from_right = lax.ppermute(from_right, axis, backward)]
    dot_general x8, matrix products: 16.5 us -> 37 us  [one(): jnp.einsum('hmqk,khe->hmqe', expo.astype(jnp.bfloat16), value_part, prefe...]
    dynamic_update_slice x0 -> x16, local copies, waits for them, and re-layouts: none -> 18.7 us  [the longest x7 9.49 us: collect(): lax.dynamic_update_slice_in_dim(out, from_right, (place + hop) % size * r...]
    dot_general x8, matrix products: 5.78 us -> 21.8 us  [one(): jnp.einsum('qhmd,khmd->hmqk', q_four, key_part, preferred_element_type=jn...]
    all_gather x1, waiting for transfers between devices: 90.3 us -> 82 us  [side_by_side(): out, at, done = (lax.all_gather(both, axis, axis=dim, tiled=True), 0, [])]
  transfers between devices with their start and end apart: 7 -> 21, of which waited for: 6 -> 15; matrix products, arithmetic and copies ran while one was open for 2% -> 8% of each run, Pallas kernels for 0% -> 0%
where the time goes in v1:
time: 412 us; the launch traced here: 411 us
  waiting for transfers between devices  207 us (50%)
  matrix products  72.7 us (18%)
  local copies, waits for them, and re-layouts  57.8 us (14%)
  starting transfers between devices  46.6 us (11%)
  between operations  14.1 us (3%)
  other arithmetic  12.5 us (3%)
    all_gather x1, waiting for transfers between devices, side_by_side(): out, at, done = (lax.all_gather(both, axis, axis=dim, tiled=True), 0, [])  82 us
    ppermute x8, waiting for transfers between devices, collect(): from_left = lax.ppermute(from_left, axis, right)  66.2 us
    reduce_scatter x1, waiting for transfers between devices, body(): lax.psum_scatter((summed + jnp.dot(y_win, proj_win, preferred_element_typ...  42.3 us
    ppermute x7, starting transfers between devices, collect(): from_right = lax.ppermute(from_right, axis, backward)  40.5 us
    dot_general x8, matrix products, one(): jnp.einsum('hmqk,khe->hmqe', expo.astype(jnp.bfloat16), value_part, prefe...  37 us
    dot_general x8, matrix products, one(): jnp.einsum('qhmd,khmd->hmqk', q_four, key_part, preferred_element_type=jn...  21.8 us
    ppermute x7, waiting for transfers between devices, collect(): from_right = lax.ppermute(from_right, axis, backward)  11.4 us
    dynamic_slice x8, local copies, waits for them, and re-layouts, body(): carry, unused = lax.scan(one, carry, (key_blocks, value_blocks))  11.3 us
  transfers between devices with their start and end apart: 21, of which 15 were waited for; matrix products, arithmetic and copies ran while one was open for 8% of the time, Pallas kernels for 0%

profile of v1, /device:TPU:40, one launch (start us, length us, event | category | flops | bytes accessed | tf_op | source)
XLA Modules:
  0.0 410.9 jit_solution(8073102060252744389)
XLA Ops:
  17.6 19.7 %collective-permute-start.1 = (bf16[256,1280]{1,0:T(8,128)(2,1)S(1)}, bf16[256,1280]{1,0:T(8,128)(2,1)}, u32[]{:S(2)}, u32[]{:S(2)}) collective-permute-start(bf16[256,1280]{1,0:T(8,128)(2,1)S(1)} %bitcast_dynamic-update-slice_fusion), channel_id=1, source_target_pairs={{0,120},{8,0},{16,8},{24,16},{32,24},{40,32},{48,40},{56,48},{64,5... | collective-permute-start | bytes 1966088 | tf_op jit(solution)/shard_map/ppermute | solution.py:30
  37.4 14.7 %collective-permute-done = bf16[256,1280]{1,0:T(8,128)(2,1)S(1)} collective-permute-done((bf16[256,1280]{1,0:T(8,128)(2,1)S(1)}, bf16[256,1280]{1,0:T(8,128)(2,1)S(1)}, u32[]{:S(2)}, u32[]{:S(2)}) %collective-permute-start) | collective-permute-done | bytes 655392 | tf_op jit(solution)/shard_map/ppermute | solution.py:27
  55.3 14.1 %collective-permute-done.2 = bf16[256,1280]{1,0:T(8,128)(2,1)} collective-permute-done((bf16[256,1280]{1,0:T(8,128)(2,1)S(1)}, bf16[256,1280]{1,0:T(8,128)(2,1)}, u32[]{:S(2)}, u32[]{:S(2)}) %collective-permute-start.2) | collective-permute-done | bytes 655392 | tf_op jit(solution)/shard_map/ppermute | solution.py:27
  72.9 13.1 %collective-permute-done.4 = bf16[256,1280]{1,0:T(8,128)(2,1)S(1)} collective-permute-done((bf16[256,1280]{1,0:T(8,128)(2,1)}, bf16[256,1280]{1,0:T(8,128)(2,1)S(1)}, u32[]{:S(2)}, u32[]{:S(2)}) %collective-permute-start.4) | collective-permute-done | bytes 655392 | tf_op jit(solution)/shard_map/ppermute | solution.py:27
  86.1 4.7 %broadcast_in_dim.24 = bf16[4096,1280]{1,0:T(8,128)(2,1)} broadcast(bf16[]{:T(256)} %constant.151.clone.1), dimensions={} | broadcast | bytes 10485762 | tf_op jit(solution)/shard_map/broadcast_in_dim | solution.py:22
  112.3 4.3 %collective-permute-done.8 = bf16[256,1280]{1,0:T(8,128)(2,1)S(1)} collective-permute-done((bf16[256,1280]{1,0:T(8,128)(2,1)S(1)}, bf16[256,1280]{1,0:T(8,128)(2,1)S(1)}, u32[]{:S(2)}, u32[]{:S(2)}) %collective-permute-start.8) | collective-permute-done | bytes 655392 | tf_op jit(solution)/shard_map/ppermute | solution.py:27
  127.1 4.4 %collective-permute-done.10 = bf16[256,1280]{1,0:T(8,128)(2,1)S(1)} collective-permute-done((bf16[256,1280]{1,0:T(8,128)(2,1)S(1)}, bf16[256,1280]{1,0:T(8,128)(2,1)S(1)}, u32[]{:S(2)}, u32[]{:S(2)}) %collective-permute-start.10) | collective-permute-done | bytes 655392 | tf_op jit(solution)/shard_map/ppermute | solution.py:27
  142.0 4.4 %collective-permute-done.12 = bf16[256,1280]{1,0:T(8,128)(2,1)S(1)} collective-permute-done((bf16[256,1280]{1,0:T(8,128)(2,1)S(1)}, bf16[256,1280]{1,0:T(8,128)(2,1)S(1)}, u32[]{:S(2)}, u32[]{:S(2)}) %collective-permute-start.12) | collective-permute-done | bytes 655392 | tf_op jit(solution)/shard_map/ppermute | solution.py:27
  151.0 7.4 %collective-permute-done.14 = bf16[256,1280]{1,0:T(8,128)(2,1)S(1)} collective-permute-done((bf16[256,1280]{1,0:T(8,128)(2,1)S(1)}, bf16[256,1280]{1,0:T(8,128)(2,1)S(1)}, u32[]{:S(2)}, u32[]{:S(2)}) %collective-permute-start.14) | collective-permute-done | bytes 655392 | tf_op jit(solution)/shard_map/ppermute | solution.py:27
  161.8 8.4 %convolution_convert_fusion = bf16[512,1280]{1,0:T(8,128)(2,1)S(1)} fusion(bf16[512,4096]{1,0:T(8,128)(2,1)S(1)} %bitcast.111, bf16[4096,1280]{1,0:T(8,128)(2,1)} %constant_dynamic-update-slice_fusion.4), kind=kOutput, calls=%fused_computation.26 | convolution fusion | flops 5369364480 | bytes 15990784 | tf_op jit(solution)/shard_map/dot_general | solution.py:106
  178.3 4.8 %collective-permute-done.16 = bf16[128,256]{1,0:T(8,128)(2,1)S(1)} collective-permute-done((bf16[128,256]{1,0:T(8,128)(2,1)}, bf16[128,256]{1,0:T(8,128)(2,1)S(1)}, u32[]{:S(2)}, u32[]{:S(2)}) %collective-permute-start.16) | collective-permute-done | bytes 65568 | tf_op jit(solution)/shard_map/ppermute | solution.py:74
  184.7 82.0 %all-gather.7.cloned.1.call-done = bf16[8192,512]{1,0:T(8,128)(2,1)} async-done(((bf16[512,512]{1,0:T(8,128)(2,1)}), bf16[8192,512]{1,0:T(8,128)(2,1)}) %all-gather.7.cloned.1.call-update) | async-done | bytes 8388624 | tf_op jit(solution)/shard_map/all_gather | solution.py:59
  266.7 5.7 %fusion.39 = (bf16[8192,256]{1,0:T(8,128)(2,1)}, bf16[8192,256]{1,0:T(8,128)(2,1)}) fusion(bf16[8192,512]{1,0:T(8,128)(2,1)} %all-gather.7.cloned.1.call-done), kind=kLoop, calls=%fused_computation.89 | loop fusion | bytes 16777216 | tf_op jit(solution)/shard_map/slice | solution.py:61
  272.4 6.9 %reshape.210 = bf16[8,1024,1,2,128]{4,3,1,0,2:T(2,128)(2,1)} reshape(bf16[8192,256]{1,0:T(8,128)(2,1)} %get-tuple-element.116) | data formatting | bytes 8388608 | tf_op jit(solution)/shard_map/reshape | solution.py:126
  279.3 76.2 %while.15 = (s32[]{:T(128)}, f32[1,2,512]{2,1,0:T(2,128)S(1)}, f32[1,2,512]{2,1,0:T(2,128)S(1)}, f32[1,2,512,256]{3,2,1,0:T(8,128)}, bf16[8,1024,1,2,128]{4,3,1,...) while((s32[]{:T(128)}, f32[1,2,512]{2,1,0:T(2,128)S(1)}, ...), condition=%wide.region_4.5_spmd.clone, body=%wide.region_1.4_spmd.clone.sunk | while | flops 814487552 | bytes 33882760 | solution.py:148
  283.5 4.3 %fusion.56 = f32[1,2,512,256]{3,2,1,0:T(8,128)} fusion(f32[2,1024,512]{2,1,0:T(8,128)} %get-tuple-element.175, f32[2,512]{1,0:T(2,128)S(1)} %bitcast.115, f32[1,2,512,256]{3,2,1,0:T(8,128)} %get-tuple-element.189, bf16[8,1024,1,256]{3,1,2,0:T(8,128)(2,1)} %get-tuple-element.201, s32[]{:T(128)} %get-tuple-element.186, ...), kind=kOutput, calls=%fused_computation.9.clone.1 | convolution fusion | flops 540803072 | bytes 6824449 | tf_op jit(solution)/shard_map/while/body/eval_jaxpr/hmqk,khe->hmqe/dot_general | solution.py:140
  292.7 4.7 %fusion.56 = f32[1,2,512,256]{3,2,1,0:T(8,128)} fusion(f32[2,1024,512]{2,1,0:T(8,128)} %get-tuple-element.175, f32[2,512]{1,0:T(2,128)S(1)} %bitcast.115, f32[1,2,512,256]{3,2,1,0:T(8,128)} %get-tuple-element.189, bf16[8,1024,1,256]{3,1,2,0:T(8,128)(2,1)} %get-tuple-element.201, s32[]{:T(128)} %get-tuple-element.186, ...), kind=kOutput, calls=%fused_computation.9.clone.1 | convolution fusion | flops 540803072 | bytes 6824449 | tf_op jit(solution)/shard_map/while/body/eval_jaxpr/hmqk,khe->hmqe/dot_general | solution.py:140
  302.3 4.7 %fusion.56 = f32[1,2,512,256]{3,2,1,0:T(8,128)} fusion(f32[2,1024,512]{2,1,0:T(8,128)} %get-tuple-element.175, f32[2,512]{1,0:T(2,128)S(1)} %bitcast.115, f32[1,2,512,256]{3,2,1,0:T(8,128)} %get-tuple-element.189, bf16[8,1024,1,256]{3,1,2,0:T(8,128)(2,1)} %get-tuple-element.201, s32[]{:T(128)} %get-tuple-element.186, ...), kind=kOutput, calls=%fused_computation.9.clone.1 | convolution fusion | flops 540803072 | bytes 6824449 | tf_op jit(solution)/shard_map/while/body/eval_jaxpr/hmqk,khe->hmqe/dot_general | solution.py:140
  311.8 4.7 %fusion.56 = f32[1,2,512,256]{3,2,1,0:T(8,128)} fusion(f32[2,1024,512]{2,1,0:T(8,128)} %get-tuple-element.175, f32[2,512]{1,0:T(2,128)S(1)} %bitcast.115, f32[1,2,512,256]{3,2,1,0:T(8,128)} %get-tuple-element.189, bf16[8,1024,1,256]{3,1,2,0:T(8,128)(2,1)} %get-tuple-element.201, s32[]{:T(128)} %get-tuple-element.186, ...), kind=kOutput, calls=%fused_computation.9.clone.1 | convolution fusion | flops 540803072 | bytes 6824449 | tf_op jit(solution)/shard_map/while/body/eval_jaxpr/hmqk,khe->hmqe/dot_general | solution.py:140
  321.4 4.7 %fusion.56 = f32[1,2,512,256]{3,2,1,0:T(8,128)} fusion(f32[2,1024,512]{2,1,0:T(8,128)} %get-tuple-element.175, f32[2,512]{1,0:T(2,128)S(1)} %bitcast.115, f32[1,2,512,256]{3,2,1,0:T(8,128)} %get-tuple-element.189, bf16[8,1024,1,256]{3,1,2,0:T(8,128)(2,1)} %get-tuple-element.201, s32[]{:T(128)} %get-tuple-element.186, ...), kind=kOutput, calls=%fused_computation.9.clone.1 | convolution fusion | flops 540803072 | bytes 6824449 | tf_op jit(solution)/shard_map/while/body/eval_jaxpr/hmqk,khe->hmqe/dot_general | solution.py:140
  331.0 4.7 %fusion.56 = f32[1,2,512,256]{3,2,1,0:T(8,128)} fusion(f32[2,1024,512]{2,1,0:T(8,128)} %get-tuple-element.175, f32[2,512]{1,0:T(2,128)S(1)} %bitcast.115, f32[1,2,512,256]{3,2,1,0:T(8,128)} %get-tuple-element.189, bf16[8,1024,1,256]{3,1,2,0:T(8,128)(2,1)} %get-tuple-element.201, s32[]{:T(128)} %get-tuple-element.186, ...), kind=kOutput, calls=%fused_computation.9.clone.1 | convolution fusion | flops 540803072 | bytes 6824449 | tf_op jit(solution)/shard_map/while/body/eval_jaxpr/hmqk,khe->hmqe/dot_general | solution.py:140
  340.6 4.7 %fusion.56 = f32[1,2,512,256]{3,2,1,0:T(8,128)} fusion(f32[2,1024,512]{2,1,0:T(8,128)} %get-tuple-element.175, f32[2,512]{1,0:T(2,128)S(1)} %bitcast.115, f32[1,2,512,256]{3,2,1,0:T(8,128)} %get-tuple-element.189, bf16[8,1024,1,256]{3,1,2,0:T(8,128)(2,1)} %get-tuple-element.201, s32[]{:T(128)} %get-tuple-element.186, ...), kind=kOutput, calls=%fused_computation.9.clone.1 | convolution fusion | flops 540803072 | bytes 6824449 | tf_op jit(solution)/shard_map/while/body/eval_jaxpr/hmqk,khe->hmqe/dot_general | solution.py:140
  350.1 4.7 %fusion.56 = f32[1,2,512,256]{3,2,1,0:T(8,128)} fusion(f32[2,1024,512]{2,1,0:T(8,128)} %get-tuple-element.175, f32[2,512]{1,0:T(2,128)S(1)} %bitcast.115, f32[1,2,512,256]{3,2,1,0:T(8,128)} %get-tuple-element.189, bf16[8,1024,1,256]{3,1,2,0:T(8,128)(2,1)} %get-tuple-element.201, s32[]{:T(128)} %get-tuple-element.186, ...), kind=kOutput, calls=%fused_computation.9.clone.1 | convolution fusion | flops 540803072 | bytes 6824449 | tf_op jit(solution)/shard_map/while/body/eval_jaxpr/hmqk,khe->hmqe/dot_general | solution.py:140
  362.1 42.3 %reduce-scatter.2.cloned.1.call-done = bf16[64,4096]{1,0:T(8,128)(2,1)} async-done(((bf16[512,4096]{1,0:T(8,128)(2,1)}), bf16[64,4096]{1,0:T(8,128)(2,1)}) %reduce-scatter.2.cloned.1.call-update) | async-done | bytes 524304 | tf_op jit(solution)/shard_map/reduce_scatter | solution.py:187
  (167 shorter events, 122.5 us)
Async XLA Ops:
  6.5 350.6 %copy-start = (bf16[256,4096]{1,0:T(8,128)(2,1)S(1)}, bf16[256,4096]{1,0:T(8,128)(2,1)}, u32[]{:S(2)}) copy-start(bf16[256,4096]{1,0:T(8,128)(2,1)} %param.24) | copy-start | bytes 6291460
  6.6 62.9 %all-gather.9.cloned.1.call-start = ((), (), s32[]{:S(2)}) async-start(), calls=%async_computation.4 | async-start | bytes 2621440 | tf_op jit(solution)/shard_map/all_gather | solution.py:46
  10.1 149.3 %all-gather.5.cloned.1.call-start = ((), (), s32[]{:S(2)}) async-start(), calls=%async_computation.1 | async-start | bytes 6291456 | tf_op jit(solution)/shard_map/all_gather | solution.py:46
  14.8 37.3 %collective-permute-start = (bf16[256,1280]{1,0:T(8,128)(2,1)S(1)}, bf16[256,1280]{1,0:T(8,128)(2,1)S(1)}, u32[]{:S(2)}, u32[]{:S(2)}) collective-permute-start(bf16[256,1280]{1,0:T(8,128)(2,1)S(1)} %bitcast_dynamic-update-slice_fusion), channel_id=1, source_target_pairs={{0,8},{8,16},{16,24},{24,32},{32,40},{40,48},{48,56},{56,64},{64,7... | collective-permute-start | bytes 1966088 | tf_op jit(solution)/shard_map/ppermute | solution.py:27
  17.6 34.4 %collective-permute-start.1 = (bf16[256,1280]{1,0:T(8,128)(2,1)S(1)}, bf16[256,1280]{1,0:T(8,128)(2,1)}, u32[]{:S(2)}, u32[]{:S(2)}) collective-permute-start(bf16[256,1280]{1,0:T(8,128)(2,1)S(1)} %bitcast_dynamic-update-slice_fusion), channel_id=1, source_target_pairs={{0,120},{8,0},{16,8},{24,16},{32,24},{40,32},{48,40},{56,48},{64,5... | collective-permute-start | bytes 1966088 | tf_op jit(solution)/shard_map/ppermute | solution.py:30
  52.1 17.4 %collective-permute-start.2 = (bf16[256,1280]{1,0:T(8,128)(2,1)S(1)}, bf16[256,1280]{1,0:T(8,128)(2,1)}, u32[]{:S(2)}, u32[]{:S(2)}) collective-permute-start(bf16[256,1280]{1,0:T(8,128)(2,1)S(1)} %collective-permute-done), channel_id=1, source_target_pairs={{0,8},{8,16},{16,24},{24,32},{32,40},{40,48},{48,56},{56,64},{64,7... | collective-permute-start | bytes 1966088 | tf_op jit(solution)/shard_map/ppermute | solution.py:27
  52.1 17.5 %collective-permute-start.3 = (bf16[256,1280]{1,0:T(8,128)(2,1)}, bf16[256,1280]{1,0:T(8,128)(2,1)}, u32[]{:S(2)}, u32[]{:S(2)}) collective-permute-start(bf16[256,1280]{1,0:T(8,128)(2,1)} %collective-permute-done.1), channel_id=1, source_target_pairs={{0,120},{8,0},{16,8},{24,16},{32,24},{40,32},{48,40},{56,48},{64,5... | collective-permute-start | bytes 1966088 | tf_op jit(solution)/shard_map/ppermute | solution.py:30
  69.4 16.6 %collective-permute-start.4 = (bf16[256,1280]{1,0:T(8,128)(2,1)}, bf16[256,1280]{1,0:T(8,128)(2,1)S(1)}, u32[]{:S(2)}, u32[]{:S(2)}) collective-permute-start(bf16[256,1280]{1,0:T(8,128)(2,1)} %collective-permute-done.2), channel_id=1, source_target_pairs={{0,8},{8,16},{16,24},{24,32},{32,40},{40,48},{48,56},{56,64},{64,7... | collective-permute-start | bytes 1966088 | tf_op jit(solution)/shard_map/ppermute | solution.py:27
  69.5 197.2 %all-gather.7.cloned.1.call-start = ((), (), s32[]{:S(2)}) async-start(), calls=%async_computation.2 | async-start | bytes 8912896 | tf_op jit(solution)/shard_map/all_gather | solution.py:59
  69.6 23.0 %collective-permute-start.5 = (bf16[256,1280]{1,0:T(8,128)(2,1)}, bf16[256,1280]{1,0:T(8,128)(2,1)}, u32[]{:S(2)}, u32[]{:S(2)}) collective-permute-start(bf16[256,1280]{1,0:T(8,128)(2,1)} %collective-permute-done.3), channel_id=1, source_target_pairs={{0,120},{8,0},{16,8},{24,16},{32,24},{40,32},{48,40},{56,48},{64,5... | collective-permute-start | bytes 1966088 | tf_op jit(solution)/shard_map/ppermute | solution.py:30
  72.9 18.7 %copy-start.5 = (bf16[256,1280]{1,0:T(8,128)(2,1)S(1)}, bf16[256,1280]{1,0:T(8,128)(2,1)}, u32[]{:S(2)}) copy-start(bf16[256,1280]{1,0:T(8,128)(2,1)} %copy-done.4) | copy-start | bytes 1966084
  86.1 15.6 %collective-permute-start.6 = (bf16[256,1280]{1,0:T(8,128)(2,1)S(1)}, bf16[256,1280]{1,0:T(8,128)(2,1)S(1)}, u32[]{:S(2)}, u32[]{:S(2)}) collective-permute-start(bf16[256,1280]{1,0:T(8,128)(2,1)S(1)} %collective-permute-done.4), channel_id=1, source_target_pairs={{0,8},{8,16},{16,24},{24,32},{32,40},{40,48},{48,56},{56,64},{64,7... | collective-permute-start | bytes 1966088 | tf_op jit(solution)/shard_map/ppermute | solution.py:27
  92.6 15.1 %collective-permute-start.7 = (bf16[256,1280]{1,0:T(8,128)(2,1)}, bf16[256,1280]{1,0:T(8,128)(2,1)S(1)}, u32[]{:S(2)}, u32[]{:S(2)}) collective-permute-start(bf16[256,1280]{1,0:T(8,128)(2,1)} %collective-permute-done.5), channel_id=1, source_target_pairs={{0,120},{8,0},{16,8},{24,16},{32,24},{40,32},{48,40},{56,48},{64,5... | collective-permute-start | bytes 1966088 | tf_op jit(solution)/shard_map/ppermute | solution.py:30
  101.6 14.9 %collective-permute-start.8 = (bf16[256,1280]{1,0:T(8,128)(2,1)S(1)}, bf16[256,1280]{1,0:T(8,128)(2,1)S(1)}, u32[]{:S(2)}, u32[]{:S(2)}) collective-permute-start(bf16[256,1280]{1,0:T(8,128)(2,1)S(1)} %collective-permute-done.6), channel_id=1, source_target_pairs={{0,8},{8,16},{16,24},{24,32},{32,40},{40,48},{48,56},{56,64},{64,7... | collective-permute-start | bytes 1966088 | tf_op jit(solution)/shard_map/ppermute | solution.py:27
  107.7 14.8 %collective-permute-start.9 = (bf16[256,1280]{1,0:T(8,128)(2,1)S(1)}, bf16[256,1280]{1,0:T(8,128)(2,1)S(1)}, u32[]{:S(2)}, u32[]{:S(2)}) collective-permute-start(bf16[256,1280]{1,0:T(8,128)(2,1)S(1)} %collective-permute-done.7), channel_id=1, source_target_pairs={{0,120},{8,0},{16,8},{24,16},{32,24},{40,32},{48,40},{56,48},{64,5... | collective-permute-start | bytes 1966088 | tf_op jit(solution)/shard_map/ppermute | solution.py:30
  116.5 14.9 %collective-permute-start.10 = (bf16[256,1280]{1,0:T(8,128)(2,1)S(1)}, bf16[256,1280]{1,0:T(8,128)(2,1)S(1)}, u32[]{:S(2)}, u32[]{:S(2)}) collective-permute-start(bf16[256,1280]{1,0:T(8,128)(2,1)S(1)} %collective-permute-done.8), channel_id=1, source_target_pairs={{0,8},{8,16},{16,24},{24,32},{32,40},{40,48},{48,56},{56,64},{64,7... | collective-permute-start | bytes 1966088 | tf_op jit(solution)/shard_map/ppermute | solution.py:27
  122.5 14.9 %collective-permute-start.11 = (bf16[256,1280]{1,0:T(8,128)(2,1)S(1)}, bf16[256,1280]{1,0:T(8,128)(2,1)S(1)}, u32[]{:S(2)}, u32[]{:S(2)}) collective-permute-start(bf16[256,1280]{1,0:T(8,128)(2,1)S(1)} %collective-permute-done.9), channel_id=1, source_target_pairs={{0,120},{8,0},{16,8},{24,16},{32,24},{40,32},{48,40},{56,48},{64,5... | collective-permute-start | bytes 1966088 | tf_op jit(solution)/shard_map/ppermute | solution.py:30
  131.4 14.9 %collective-permute-start.12 = (bf16[256,1280]{1,0:T(8,128)(2,1)S(1)}, bf16[256,1280]{1,0:T(8,128)(2,1)S(1)}, u32[]{:S(2)}, u32[]{:S(2)}) collective-permute-start(bf16[256,1280]{1,0:T(8,128)(2,1)S(1)} %collective-permute-done.10), channel_id=1, source_target_pairs={{0,8},{8,16},{16,24},{24,32},{32,40},{40,48},{48,56},{56,64},{64,7... | collective-permute-start | bytes 1966088 | tf_op jit(solution)/shard_map/ppermute | solution.py:27
  137.4 12.7 %collective-permute-start.13 = (bf16[256,1280]{1,0:T(8,128)(2,1)S(1)}, bf16[256,1280]{1,0:T(8,128)(2,1)S(1)}, u32[]{:S(2)}, u32[]{:S(2)}) collective-permute-start(bf16[256,1280]{1,0:T(8,128)(2,1)S(1)} %collective-permute-done.11), channel_id=1, source_target_pairs={{0,120},{8,0},{16,8},{24,16},{32,24},{40,32},{48,40},{56,48},{64,5... | collective-permute-start | bytes 1966088 | tf_op jit(solution)/shard_map/ppermute | solution.py:30
  146.3 12.1 %collective-permute-start.14 = (bf16[256,1280]{1,0:T(8,128)(2,1)S(1)}, bf16[256,1280]{1,0:T(8,128)(2,1)S(1)}, u32[]{:S(2)}, u32[]{:S(2)}) collective-permute-start(bf16[256,1280]{1,0:T(8,128)(2,1)S(1)} %collective-permute-done.12), channel_id=1, source_target_pairs={{0,8},{8,16},{16,24},{24,32},{32,40},{40,48},{48,56},{56,64},{64,7... | collective-permute-start | bytes 1966088 | tf_op jit(solution)/shard_map/ppermute | solution.py:27
  171.3 233.1 %reduce-scatter.2.cloned.1.call-start = ((), (), s32[]{:S(2)}) async-start(), calls=%async_computation.3 | async-start | bytes 4718592 | tf_op jit(solution)/shard_map/reduce_scatter | solution.py:187
  173.8 4.5 %collective-permute-start.15 = (bf16[128,256]{1,0:T(8,128)(2,1)}, bf16[128,256]{1,0:T(8,128)(2,1)S(1)}, u32[]{:S(2)}, u32[]{:S(2)}) collective-permute-start(bf16[128,256]{1,0:T(8,128)(2,1)} %get-tuple-element.120), channel_id=1, source_target_pairs={{0,8},{8,16},{16,24},{24,32},{32,40},{40,48},{48,56},{56,64},{64,7... | collective-permute-start | bytes 196616 | tf_op jit(solution)/shard_map/ppermute | solution.py:73
  175.3 7.9 %collective-permute-start.16 = (bf16[128,256]{1,0:T(8,128)(2,1)}, bf16[128,256]{1,0:T(8,128)(2,1)S(1)}, u32[]{:S(2)}, u32[]{:S(2)}) collective-permute-start(bf16[128,256]{1,0:T(8,128)(2,1)} %get-tuple-element.121), channel_id=1, source_target_pairs={{8,0},{16,8},{24,16},{32,24},{40,32},{48,40},{56,48},{64,56},{72,6... | collective-permute-start | bytes 196616 | tf_op jit(solution)/shard_map/ppermute | solution.py:74
  279.3 77.9 %copy-start.7 = (f32[256]{0:T(256)S(1)}, f32[256]{0:T(256)}, u32[]{:S(2)}) copy-start(f32[256]{0:T(256)} %param.20) | copy-start | bytes 3076
  (13 other events, 63.2 us)
Sparse Core Ops, SparseCore 0:
  10.2 50.0 all-gather.8
  69.6 17.3 all-gather.4
  171.4 95.2 all-gather.6
  362.2 42.0 reduce-scatter.1
